TPU v7x, 32 devices: a whole 2x2x4 slice. The times are simulated.
32 devices in a mesh: rep: 2 (over x), fs: 8 (over z, y), tp: 2 (over core).
Axes of the slice: x: 2, y: 2, z: 4, core: 2. Of those that a mesh axis runs over, the one named last changes fastest.
Arguments:
- pre_gate: bfloat16 [12288, 4096], P(('rep', 'fs'), 'tp'), may hold values from -6 to 6
- pre_linear: bfloat16 [12288, 4096], P(('rep', 'fs'), 'tp'), may hold values from -6 to 6
- taps_gate: float32 [3, 4096], P(None, 'tp'), may hold values from -3.5 to 3.5
- taps_linear: float32 [3, 4096], P(None, 'tp'), may hold values from -3.5 to 3.5
- bias_gate: float32 [4096], P('tp'), may hold values from -3 to 3
- bias_linear: float32 [4096], P('tp'), may hold values from -3 to 3
- down_weight: bfloat16 [4096, 2048], P('tp', 'fs'), may hold values from -0.09375 to 0.09375
- out_grad: bfloat16 [12288, 2048], P(('rep', 'fs')), may hold values from -8 to 8
Outputs:
- grad_gate: bfloat16 [12288, 4096], P(('rep', 'fs'), 'tp')
- grad_linear: bfloat16 [12288, 4096], P(('rep', 'fs'), 'tp')
- grad_taps_gate: float32 [3, 4096], P(None, 'tp')
- grad_taps_linear: float32 [3, 4096], P(None, 'tp')
- grad_bias_gate: float32 [4096], P('tp')
- grad_bias_linear: float32 [4096], P('tp')
- grad_down: float32 [4096, 2048], P('tp', 'fs')
- row_norms: float32 [4096], P('tp')
All inputs are finite; a program needn't handle non-finite values.
Results may differ from a plain program's by a relative error of at most 0.0031.
Values may be sent and summed in bfloat16 or wider, within the bound.
A program may use at most 128 MiB of HBM per device.

v0:
```python
import functools

import jax
import jax.numpy as jnp
from jax import lax
from jax.experimental import pallas as pl
from jax.experimental.pallas import tpu as pltpu
from jax.sharding import PartitionSpec as P

MESH = pl.DeviceIdType.MESH


def shift_down(values, steps):
    if steps == 0:
        return values
    rows = lax.broadcasted_iota(jnp.int32, values.shape, 0)
    return jnp.where(rows < steps, 0.0, pltpu.roll(values, steps, 0))


def shift_up(values, steps):
    length = values.shape[0]
    rows = lax.broadcasted_iota(jnp.int32, values.shape, 0)
    return jnp.where(rows >= length - steps, 0.0, pltpu.roll(values, length - steps, 0))


def conv_chunk(values, taps, bias):
    return (
        taps[0:1] * shift_down(values, 2)
        + taps[1:2] * shift_down(values, 1)
        + taps[2:3] * values
        + bias
    )


def conv_back_chunk(grads, taps):
    return taps[0:1] * shift_up(grads, 2) + taps[1:2] * shift_up(grads, 1) + taps[2:3] * grads


def kernel(
    fs, chunk,
    pg_ref, pl_ref, tg_ref, tl_ref, bg_ref, bl_ref, w_ref, og_ref,
    gg_ref, gl_ref, cp_ref, gd_ref, rn_ref,
    wbuf, sbuf, pbuf, rbuf, xs, xr, cpbuf, cps, cpx, rnbuf,
    w_send, w_recv, y_send, y_recv, p_send, p_recv, f_send, f_recv, s_send, s_recv, x_send, x_recv,
    c_send, c_recv, cx_send, cx_recv, n_send, n_recv,
):
    me = lax.axis_index("fs")
    rep = lax.axis_index("rep")
    partner = 1 - rep
    pairs = fs // 2
    z = me // 2
    par = me % 2
    mate = me + 1 - 2 * par
    tokens, ff = pg_ref.shape
    dc = w_ref.shape[1]
    chunks = ff // chunk
    half = ff // 2
    lag = chunks // 2
    per = -(-(fs - 1) // chunks)

    def to(k):
        return lax.rem(me + k, fs)

    def rows_of(c):
        return pl.ds(pl.multiple_of(c * chunk, chunk), chunk)

    def shard(z_at, parity):
        return z_at * 2 + parity

    def z_to(k):
        return lax.rem(z + k, pairs)

    def z_from(k):
        return lax.rem(z + pairs - k, pairs)

    def my_half():
        return pl.ds(pl.multiple_of(rep * half, half), half)

    def w_copy(k):
        return pltpu.make_async_remote_copy(
            src_ref=w_ref.at[my_half()], dst_ref=wbuf.at[me, my_half()],
            send_sem=w_send.at[k], recv_sem=w_recv.at[k],
            device_id={"fs": shard(z_to(k), par)}, device_id_type=MESH)

    def y_first():
        return pltpu.make_async_remote_copy(
            src_ref=w_ref.at[my_half()], dst_ref=wbuf.at[me, my_half()],
            send_sem=y_send.at[0], recv_sem=y_recv.at[0],
            device_id={"fs": mate}, device_id_type=MESH)

    def y_copy(k):
        block = wbuf.at[shard(z_from(k), par), my_half()]
        return pltpu.make_async_remote_copy(
            src_ref=block, dst_ref=block,
            send_sem=y_send.at[k], recv_sem=y_recv.at[k],
            device_id={"fs": mate}, device_id_type=MESH)

    def f_copy(item):
        block = wbuf.at[shard(z_from(item % pairs), (par + item // pairs) % 2), my_half()]
        return pltpu.make_async_remote_copy(
            src_ref=block, dst_ref=block,
            send_sem=f_send.at[item], recv_sem=f_recv.at[item],
            device_id={"rep": partner}, device_id_type=MESH)

    def p_copy(c):
        return pltpu.make_async_remote_copy(
            src_ref=sbuf.at[1 - par, :, rows_of(c)], dst_ref=pbuf.at[:, rows_of(c)],
            send_sem=p_send.at[c], recv_sem=p_recv.at[c],
            device_id={"fs": mate}, device_id_type=MESH)

    def s_copy(c, k):
        return pltpu.make_async_remote_copy(
            src_ref=sbuf.at[par, z_to(k), rows_of(c)], dst_ref=rbuf.at[k, rows_of(c)],
            send_sem=s_send.at[c, k], recv_sem=s_recv.at[c, k],
            device_id={"fs": shard(z_to(k), par)}, device_id_type=MESH)

    def pair_sum(c):
        p_copy(c).wait_recv()
        for at in range(pairs):
            both = sbuf[par, at, rows_of(c)].astype(jnp.float32) + pbuf[at, rows_of(c)].astype(jnp.float32)
            sbuf[par, at, rows_of(c)] = both.astype(jnp.bfloat16)

        @pl.loop(1, pairs)
        def _(k):
            s_copy(c, k).start()

    def x_copy(c):
        return pltpu.make_async_remote_copy(
            src_ref=xs.at[rows_of(c)], dst_ref=xr.at[rows_of(c)],
            send_sem=x_send.at[c], recv_sem=x_recv.at[c],
            device_id={"rep": partner}, device_id_type=MESH)

    def c_copy(k):
        return pltpu.make_async_remote_copy(
            src_ref=cpbuf.at[me], dst_ref=cpbuf.at[me],
            send_sem=c_send.at[k], recv_sem=c_recv.at[k],
            device_id={"fs": to(k)}, device_id_type=MESH)

    def cx_copy():
        return pltpu.make_async_remote_copy(
            src_ref=cps, dst_ref=cpx, send_sem=cx_send, recv_sem=cx_recv,
            device_id={"rep": partner}, device_id_type=MESH)

    def n_copy(k):
        return pltpu.make_async_remote_copy(
            src_ref=rnbuf.at[me], dst_ref=rnbuf.at[me],
            send_sem=n_send.at[k], recv_sem=n_recv.at[k],
            device_id={"fs": to(k)}, device_id_type=MESH)

    barrier = pltpu.get_barrier_semaphore()

    @pl.loop(1, fs)
    def _(k):
        pl.semaphore_signal(barrier, inc=1, device_id={"fs": to(k)}, device_id_type=MESH)

    pl.semaphore_signal(barrier, inc=1, device_id={"rep": partner}, device_id_type=MESH)
    pl.semaphore_wait(barrier, fs)

    y_first().start()

    @pl.loop(1, pairs)
    def _(k):
        w_copy(k).start()

    wbuf[me] = w_ref[...]

    @pl.loop(0, chunks)
    def _(c):
        cols = rows_of(c)
        gate_pre = conv_chunk(
            pg_ref[:, cols].astype(jnp.float32), tg_ref[:, cols], bg_ref[:, cols])
        linear_pre = conv_chunk(
            pl_ref[:, cols].astype(jnp.float32), tl_ref[:, cols], bl_ref[:, cols])
        hidden = (gate_pre * jax.nn.sigmoid(gate_pre) * linear_pre).astype(jnp.bfloat16)
        for j in range(fs):
            part = lax.dot_general(
                hidden, og_ref[:, j * dc:(j + 1) * dc], (((0,), (0,)), ((), ())),
                preferred_element_type=jnp.float32)
            sbuf[j % 2, j // 2, cols] = part.astype(jnp.bfloat16)

        p_copy(c).start()

        @pl.when(c >= lag)
        def _():
            pair_sum(c - lag)

        for step in range(per):
            k = c * per + step + 1

            @pl.when(k < pairs)
            def _():
                w_copy(k).wait_recv()
                y_copy(k).start()
                f_copy(k).start()

            @pl.when((k >= pairs) & (k < fs))
            def _():
                y_copy(k - pairs).wait_recv()
                f_copy(k).start()

    @pl.loop(1, fs)
    def _(k):
        f_copy(k).wait_recv()

    @pl.loop(0, chunks)
    def _(c):
        cols = rows_of(c)
        gate_in = pg_ref[:, cols].astype(jnp.float32)
        linear_in = pl_ref[:, cols].astype(jnp.float32)
        taps_gate, taps_linear = tg_ref[:, cols], tl_ref[:, cols]
        gate_pre = conv_chunk(gate_in, taps_gate, bg_ref[:, cols])
        linear_pre = conv_chunk(linear_in, taps_linear, bl_ref[:, cols])
        sigma = jax.nn.sigmoid(gate_pre)
        grad_hidden = jnp.zeros((tokens, chunk), jnp.float32)
        for j in range(fs):
            grad_hidden += lax.dot_general(
                og_ref[:, j * dc:(j + 1) * dc], wbuf[j, cols], (((1,), (1,)), ((), ())),
                preferred_element_type=jnp.float32)
        grad_gate_pre = grad_hidden * linear_pre * sigma * (1.0 + gate_pre * (1.0 - sigma))
        grad_linear_pre = grad_hidden * (gate_pre * sigma)
        gg_ref[:, cols] = conv_back_chunk(grad_gate_pre, taps_gate).astype(jnp.bfloat16)
        gl_ref[:, cols] = conv_back_chunk(grad_linear_pre, taps_linear).astype(jnp.bfloat16)
        for j in range(3):
            cpbuf[me, j:j + 1, cols] = jnp.sum(
                grad_gate_pre * shift_down(gate_in, 2 - j), axis=0, keepdims=True)
            cpbuf[me, j + 3:j + 4, cols] = jnp.sum(
                grad_linear_pre * shift_down(linear_in, 2 - j), axis=0, keepdims=True)
        cpbuf[me, 6:7, cols] = jnp.sum(grad_gate_pre, axis=0, keepdims=True)
        cpbuf[me, 7:8, cols] = jnp.sum(grad_linear_pre, axis=0, keepdims=True)

        @pl.when(c == chunks - 1)
        def _():
            @pl.loop(1, fs)
            def _(k):
                c_copy(k).start()

        @pl.when(c < lag)
        def _():
            pair_sum(chunks - lag + c)

        total = sbuf[par, z, cols].astype(jnp.float32)
        for k in range(1, pairs):
            s_copy(c, k).wait_recv()
            total += rbuf[k, cols].astype(jnp.float32)
        xs[cols] = total
        x_copy(c).start()

    @pl.loop(1, fs)
    def _(k):
        c_copy(k).wait_recv()

    sums = cpbuf[0]
    for j in range(1, fs):
        sums += cpbuf[j]
    cps[...] = sums
    cx_copy().start()

    @pl.loop(0, chunks)
    def _(c):
        rows = rows_of(c)
        x_copy(c).wait_recv()
        total = xs[rows] + xr[rows]
        gd_ref[rows] = total
        square = total * total
        while square.shape[1] % 256 == 0:
            middle = square.shape[1] // 2
            square = square[:, :middle] + square[:, middle:]
        rnbuf[me, 0:1, rows] = jnp.sum(square.T, axis=0, keepdims=True)

    @pl.loop(1, fs)
    def _(k):
        n_copy(k).start()

    cx_copy().wait_recv()
    cp_ref[...] = cps[...] + cpx[...]

    @pl.loop(1, fs)
    def _(k):
        n_copy(k).wait_recv()

    norms = rnbuf[0]
    for j in range(1, fs):
        norms += rnbuf[j]
    rn_ref[...] = norms

    cx_copy().wait_send()
    y_first().wait_send()

    @pl.loop(1, pairs)
    def _(k):
        w_copy(k).wait_send()
        y_copy(k).wait_send()

    @pl.loop(1, fs)
    def _(k):
        f_copy(k).wait_send()
        c_copy(k).wait_send()
        n_copy(k).wait_send()

    @pl.loop(0, chunks)
    def _(c):
        x_copy(c).wait_send()
        p_copy(c).wait_send()

        @pl.loop(1, pairs)
        def _(k):
            s_copy(c, k).wait_send()


def local(
    fs, pre_gate, pre_linear, taps_gate, taps_linear, bias_gate, bias_linear, down_weight, out_grad
):
    tokens, ff = pre_gate.shape
    dc = down_weight.shape[1]
    chunk = 256
    chunks = ff // chunk
    pairs = fs // 2
    f32, bf16 = jnp.float32, jnp.bfloat16
    vmem = pl.BlockSpec(memory_space=pltpu.VMEM)
    dma = pltpu.SemaphoreType.DMA
    gg, gl, cp, gd, rn = pl.pallas_call(
        functools.partial(kernel, fs, chunk),
        out_shape=(
            jax.ShapeDtypeStruct((tokens, ff), bf16),
            jax.ShapeDtypeStruct((tokens, ff), bf16),
            jax.ShapeDtypeStruct((8, ff), f32),
            jax.ShapeDtypeStruct((ff, dc), f32),
            jax.ShapeDtypeStruct((1, ff), f32),
        ),
        in_specs=[vmem] * 8,
        out_specs=(vmem,) * 5,
        scratch_shapes=[
            pltpu.VMEM((fs, ff, dc), bf16),
            pltpu.VMEM((2, pairs, ff, dc), bf16),
            pltpu.VMEM((pairs, ff, dc), bf16),
            pltpu.VMEM((pairs, ff, dc), bf16),
            pltpu.VMEM((ff, dc), f32),
            pltpu.VMEM((ff, dc), f32),
            pltpu.VMEM((fs, 8, ff), f32),
            pltpu.VMEM((8, ff), f32),
            pltpu.VMEM((8, ff), f32),
            pltpu.VMEM((fs, 1, ff), f32),
            dma((pairs,)), dma((pairs,)), dma((pairs,)), dma((pairs,)),
            dma((chunks,)), dma((chunks,)), dma((fs,)), dma((fs,)),
            dma((chunks, pairs)), dma((chunks, pairs)), dma((chunks,)), dma((chunks,)),
            dma((fs,)), dma((fs,)), dma, dma, dma((fs,)), dma((fs,)),
        ],
        compiler_params=pltpu.CompilerParams(
            collective_id=0, has_side_effects=True, vmem_limit_bytes=67043328),
    )(pre_gate, pre_linear, taps_gate, taps_linear, bias_gate[None], bias_linear[None],
      down_weight, out_grad)
    return gg, gl, cp[0:3], cp[3:6], cp[6], cp[7], gd, rn[0]


def solution(mesh):
    in_specs = (
        P(("rep", "fs"), "tp"),
        P(("rep", "fs"), "tp"),
        P(None, "tp"),
        P(None, "tp"),
        P("tp"),
        P("tp"),
        P("tp", "fs"),
        P(("rep", "fs"), None),
    )
    out_specs = (
        P(("rep", "fs"), "tp"),
        P(("rep", "fs"), "tp"),
        P(None, "tp"),
        P(None, "tp"),
        P("tp"),
        P("tp"),
        P("tp", "fs"),
        P("tp"),
    )
    return jax.shard_map(
        functools.partial(local, mesh.shape["fs"]), mesh=mesh, in_specs=in_specs, out_specs=out_specs, check_vma=False)
```

profile of v0, /device:TPU:0, one launch (start us, length us, event | category | flops | bytes accessed | tf_op | source)
XLA Modules:
  0.0 200.1 jit_solution(16658635276145665691)
XLA Ops:
  0.6 187.6 %shard_map.143 = (bf16[768,2048]{1,0:T(8,128)(2,1)}, bf16[768,2048]{1,0:T(8,128)(2,1)}, f32[8,2048]{1,0:T(8,128)}, f32[2048,256]{1,0:T(8,128)}, f32[1,2048]{1,0:T(1,128)}) custom-call(bf16[768,2048]{1,0:T(8,128)(2,1)} %pg_ref.1, bf16[768,2048]{1,0:T(8,128)(2,1)} %pl_ref.1, f32[3,2048]{1,0:T(4,128)} %tg_ref.1, f32[3,2048]{1,0:T(4,128)} %tl_ref.1, ...), custom_call_target="tpu_custom_call" | custom-call | tf_op jit(solution)/shard_map/pallas_call | solution.py:321
  188.3 1.6 fusion.1
  189.8 1.5 fusion
  191.4 0.0 copy-start
  191.4 4.1 %copy.20 = bf16[768,2048]{1,0:T(8,128)(2,1)} copy(bf16[768,2048]{1,0:T(8,128)(2,1)} %get-tuple-element.30) | data formatting | bytes 6291456
  195.5 0.0 copy-done
  195.5 0.0 copy-start.1
  195.5 1.7 copy.21
  197.1 1.1 copy-done.1
  198.2 0.0 copy-start.2
  198.2 1.3 copy.22
  199.5 0.0 copy-done.2
  199.5 0.6 copy.23
Async XLA Ops:
  191.4 4.1 %copy-start = (bf16[768,2048]{1,0:T(8,128)(2,1)S(1)}, bf16[768,2048]{1,0:T(8,128)(2,1)}, u32[]{:S(2)}) copy-start(bf16[768,2048]{1,0:T(8,128)(2,1)} %get-tuple-element.31) | copy-start | bytes 9437188
  195.5 2.7 %copy-start.1 = (f32[2048,256]{1,0:T(8,128)S(1)}, f32[2048,256]{1,0:T(8,128)}, u32[]{:S(2)}) copy-start(f32[2048,256]{1,0:T(8,128)} %get-tuple-element.36) | copy-start | bytes 6291460
  198.2 1.3 copy-start.2
where the time goes:
time: 200 us
  Pallas kernels  188 us (94%)
  local copies, waits for them, and re-layouts  11.8 us (6%)
    pallas_call x1, Pallas kernels, local(): pl.pallas_call(functools.partial(kernel, fs, chunk), out_shape=(jax.Shape...  188 us
    unnamed x10, local copies, waits for them, and re-layouts  8.77 us

commit v1 on v0

--- a/solution.py
+++ b/solution.py
@@ -307,6 +307,42 @@
             s_copy(c, k).wait_send()
 
 
+def out_kernel(gg, gl, cp, gd, rn, ogg, ogl, otg, otl, obg, obl, ogd, orn, sem):
+    copies = [
+        pltpu.make_async_copy(source, target, sem.at[i])
+        for i, (source, target) in enumerate(((gg, ogg), (gl, ogl), (gd, ogd)))
+    ]
+    for copy in copies:
+        copy.start()
+    otg[...] = cp[0:3]
+    otl[...] = cp[3:6]
+    obg[...] = cp[6:7]
+    obl[...] = cp[7:8]
+    orn[...] = rn[...]
+    for copy in copies:
+        copy.wait()
+
+
+def put_out(gg, gl, cp, gd, rn):
+    ff = gg.shape[1]
+    f32 = jnp.float32
+    vmem = pl.BlockSpec(memory_space=pltpu.VMEM)
+    hbm = pl.BlockSpec(memory_space=pl.ANY)
+    row = jax.ShapeDtypeStruct((1, ff), f32)
+    taps = jax.ShapeDtypeStruct((3, ff), f32)
+    ogg, ogl, otg, otl, obg, obl, ogd, orn = pl.pallas_call(
+        out_kernel,
+        out_shape=(
+            jax.ShapeDtypeStruct(gg.shape, gg.dtype), jax.ShapeDtypeStruct(gl.shape, gl.dtype),
+            taps, taps, row, row, jax.ShapeDtypeStruct(gd.shape, gd.dtype), row),
+        in_specs=[vmem] * 5,
+        out_specs=(hbm, hbm, vmem, vmem, vmem, vmem, hbm, vmem),
+        scratch_shapes=[pltpu.SemaphoreType.DMA((3,))],
+        compiler_params=pltpu.CompilerParams(vmem_limit_bytes=2 << 20),
+    )(*[pltpu.with_memory_space_constraint(value, pltpu.VMEM) for value in (gg, gl, cp, gd, rn)])
+    return ogg, ogl, otg, otl, obg[0], obl[0], ogd, orn[0]
+
+
 def local(
     fs, pre_gate, pre_linear, taps_gate, taps_linear, bias_gate, bias_linear, down_weight, out_grad
 ):
@@ -321,11 +357,11 @@
     gg, gl, cp, gd, rn = pl.pallas_call(
         functools.partial(kernel, fs, chunk),
         out_shape=(
-            jax.ShapeDtypeStruct((tokens, ff), bf16),
-            jax.ShapeDtypeStruct((tokens, ff), bf16),
-            jax.ShapeDtypeStruct((8, ff), f32),
-            jax.ShapeDtypeStruct((ff, dc), f32),
-            jax.ShapeDtypeStruct((1, ff), f32),
+            pltpu.VMEM((tokens, ff), bf16),
+            pltpu.VMEM((tokens, ff), bf16),
+            pltpu.VMEM((8, ff), f32),
+            pltpu.VMEM((ff, dc), f32),
+            pltpu.VMEM((1, ff), f32),
         ),
         in_specs=[vmem] * 8,
         out_specs=(vmem,) * 5,
@@ -346,10 +382,10 @@
             dma((fs,)), dma((fs,)), dma, dma, dma((fs,)), dma((fs,)),
         ],
         compiler_params=pltpu.CompilerParams(
-            collective_id=0, has_side_effects=True, vmem_limit_bytes=67043328),
+            collective_id=0, has_side_effects=True, vmem_limit_bytes=52 << 20),
     )(pre_gate, pre_linear, taps_gate, taps_linear, bias_gate[None], bias_linear[None],
       down_weight, out_grad)
-    return gg, gl, cp[0:3], cp[3:6], cp[6], cp[7], gd, rn[0]
+    return put_out(gg, gl, cp, gd, rn)
 
 
 def solution(mesh):

time: 200 us -> 189 us (0.945)
  local copies, waits for them, and re-layouts: 11.8 us -> 0 us
    unnamed x10 -> x0, local copies, waits for them, and re-layouts: 8.77 us -> none
    slice x2 -> x0, local copies, waits for them, and re-layouts: 3.08 us -> none  [local(): return (gg, gl, cp[0:3], cp[3:6], cp[6], cp[7], gd, rn[0])]
    pallas_call x1 -> x2, Pallas kernels: 188 us -> 188 us  [the longest x1 184 us: local(): pl.pallas_call(functools.partial(kernel, fs, chunk), out_shape=(pltpu.VME...]
where the time goes in v1:
time: 189 us
  Pallas kernels  188 us (99%)
    pallas_call x1, Pallas kernels, local(): pl.pallas_call(functools.partial(kernel, fs, chunk), out_shape=(pltpu.VME...  184 us
    pallas_call x1, Pallas kernels, put_out(): pl.pallas_call(out_kernel, out_shape=(jax.ShapeDtypeStruct(gg.shape, gg.d...  4.05 us

profile of v1, /device:TPU:0, one launch (start us, length us, event | category | flops | bytes accessed | tf_op | source)
XLA Modules:
  0.0 189.1 jit_solution(5046277301565706891)
XLA Ops:
  0.6 184.4 %shard_map.143 = (bf16[768,2048]{1,0:T(8,128)(2,1)S(1)}, bf16[768,2048]{1,0:T(8,128)(2,1)S(1)}, f32[8,2048]{1,0:T(8,128)S(1)}, f32[2048,256]{1,0:T(8,128)S(1)}, f32[1,2048]{1,0:T(1,128)S(1)}) custom-call(bf16[768,2048]{1,0:T(8,128)(2,1)} %pg_ref.1, bf16[768,2048]{1,0:T(8,128)(2,1)} %pl_ref.1, f32[3,2048]{1,0:T(4,128)} %tg_ref.1, f32[3,2048]{1,0:T(4,128)} %tl_ref.1, ...), custom_call_target="tpu_custom_call" | custom-call | tf_op jit(solution)/shard_map/pallas_call | solution.py:357
  185.1 4.1 %shard_map.144 = (bf16[768,2048]{1,0:T(8,128)(2,1)}, bf16[768,2048]{1,0:T(8,128)(2,1)}, f32[3,2048]{1,0:T(4,128)}, f32[3,2048]{1,0:T(4,128)}, f32[1,2048]{1,0:T(...) custom-call(bf16[768,2048]{1,0:T(8,128)(2,1)S(1)} %get-tuple-element.21.gg, ...), custom_call_target="tpu_custom_call" | custom-call | tf_op jit(solution)/shard_map/pallas_call | solution.py:333

commit v2 on v1

--- a/solution.py
+++ b/solution.py
@@ -318,7 +318,9 @@
     otl[...] = cp[3:6]
     obg[...] = cp[6:7]
     obl[...] = cp[7:8]
-    orn[...] = rn[...]
+    width = rn.shape[1]
+    for i in range(rn.shape[0]):
+        orn[0:1, i * width:(i + 1) * width] = rn[i:i + 1]
     for copy in copies:
         copy.wait()
 
@@ -343,7 +345,7 @@
     return ogg, ogl, otg, otl, obg[0], obl[0], ogd, orn[0]
 
 
-def local(
+def direct_local(
     fs, pre_gate, pre_linear, taps_gate, taps_linear, bias_gate, bias_linear, down_weight, out_grad
 ):
     tokens, ff = pre_gate.shape
@@ -388,6 +390,463 @@
     return put_out(gg, gl, cp, gd, rn)
 
 
+def line_kernel(
+    fs, unit,
+    pg_hbm, pl_hbm, tg_ref, tl_ref, bg_ref, bl_ref, w_hbm, og_hbm,
+    gg_ref, gl_ref, cp_ref, gd_ref, rn_ref,
+    og, pg, pln, wbuf, xs, xr, own, zb, ys, yr, cpl, cpr, cps, rnb,
+    in_sem, og_sem, w_sem, x_send, x_recv, wz_send, wz_recv, wy_send, wy_recv,
+    zu_send, zu_recv, zd_send, zd_recv, y_send, y_recv, a_send, a_recv,
+    c_send, c_recv, b_send, b_recv, n_send, n_recv,
+):
+    me = lax.axis_index("fs")
+    rep = lax.axis_index("rep")
+    partner = 1 - rep
+    nz = fs // 2
+    peers = 2 * fs
+    z = me // 2
+    y = me % 2
+    mate = me + 1 - 2 * y
+    flat = rep * fs + me
+    tokens, ff = pg_hbm.shape
+    dc = w_hbm.shape[1]
+    units = ff // unit
+    half = unit // 2
+    chunks = 2 * units
+    ch = half // 2
+    span = ff // peers
+    wch = unit // 2
+
+    def unit_cols(u):
+        return pl.ds(pl.multiple_of(u * unit, unit), unit)
+
+    def half_cols(u, side):
+        return pl.ds(pl.multiple_of(u * unit + side * half, half), half)
+
+    def chunk_rows(c, side):
+        start = (c // 2) * unit + side * half + (c % 2) * ch
+        return pl.ds(pl.multiple_of(start, ch), ch)
+
+    def w_rows(k):
+        return pl.ds(pl.multiple_of(k * wch, wch), wch)
+
+    def peer(k):
+        at = lax.rem(flat + k, peers)
+        return {"rep": at // fs, "fs": at % fs}
+
+    def remote(source, target, send, recv, device):
+        return pltpu.make_async_remote_copy(
+            src_ref=source, dst_ref=target, send_sem=send, recv_sem=recv,
+            device_id=device, device_id_type=MESH)
+
+    def in_copies(u):
+        cols = unit_cols(u)
+        return (
+            pltpu.make_async_copy(pg_hbm.at[:, cols], pg.at[:, cols], in_sem.at[0, u]),
+            pltpu.make_async_copy(pl_hbm.at[:, cols], pln.at[:, cols], in_sem.at[1, u]))
+
+    def og_copy():
+        return pltpu.make_async_copy(og_hbm, og, og_sem)
+
+    def w_copy():
+        return pltpu.make_async_copy(w_hbm, wbuf.at[me], w_sem)
+
+    def x_copy(c):
+        return remote(xs.at[c], xr.at[c], x_send.at[c], x_recv.at[c], {"rep": partner})
+
+    def wz_copy(way, k, src):
+        block = wbuf.at[src * 2 + y, w_rows(k)]
+        to = z + 1 if way == 0 else z - 1
+        return remote(block, block, wz_send.at[way, k, src], wz_recv.at[k, src], {"fs": to * 2 + y})
+
+    def wy_copy(k, src):
+        block = wbuf.at[src * 2 + y, w_rows(k)]
+        return remote(block, block, wy_send.at[k, src], wy_recv.at[k, src], {"fs": mate})
+
+    def z_up(c, i):
+        return remote(
+            zb.at[c, i], zb.at[c, i], zu_send.at[c, i], zu_recv.at[c, i], {"fs": (z + 1) * 2 + y})
+
+    def z_down(c, i):
+        slot = jnp.where(i == z - 1, nz, i)
+        return remote(
+            zb.at[c, i], zb.at[c, slot], zd_send.at[c, i], zd_recv.at[c, i], {"fs": (z - 1) * 2 + y})
+
+    def y_copy(c):
+        return remote(ys.at[c], yr.at[c], y_send.at[c], y_recv.at[c], {"fs": mate})
+
+    def a_copy(c):
+        rows = chunk_rows(c, rep)
+        return remote(gd_ref.at[rows], gd_ref.at[rows], a_send.at[c], a_recv.at[c], {"rep": partner})
+
+    def c_copy(k):
+        at = lax.rem(flat + k, peers)
+        cols = pl.ds(pl.multiple_of(at * span, span), span)
+        return remote(cpl.at[:, cols], cpr.at[flat], c_send.at[k], c_recv.at[k], peer(k))
+
+    def my_span():
+        return pl.ds(pl.multiple_of(flat * span, span), span)
+
+    def b_copy(k):
+        return remote(cps, cp_ref.at[:, my_span()], b_send.at[k], b_recv.at[k], peer(k))
+
+    def n_copy(k):
+        return remote(rnb.at[flat], rnb.at[flat], n_send.at[k], n_recv.at[k], peer(k))
+
+    barrier = pltpu.get_barrier_semaphore()
+
+    @pl.loop(1, peers)
+    def _(k):
+        pl.semaphore_signal(barrier, inc=1, device_id=peer(k), device_id_type=MESH)
+
+    w_copy().start()
+    for copy in in_copies(0):
+        copy.start()
+    og_copy().start()
+
+    @pl.loop(1, units)
+    def _(u):
+        for copy in in_copies(u):
+            copy.start()
+
+    w_copy().wait()
+    pl.semaphore_wait(barrier, peers - 1)
+
+    def hidden_half(cols):
+        gate_pre = conv_chunk(pg[:, cols].astype(jnp.float32), tg_ref[:, cols], bg_ref[:, cols])
+        linear_pre = conv_chunk(pln[:, cols].astype(jnp.float32), tl_ref[:, cols], bl_ref[:, cols])
+        return (gate_pre * jax.nn.sigmoid(gate_pre) * linear_pre).astype(jnp.bfloat16)
+
+    def forward(u):
+        for copy in in_copies(u):
+            copy.wait()
+        hidden = jnp.concatenate(
+            [hidden_half(half_cols(u, rep)), hidden_half(half_cols(u, partner))], axis=1)
+        for j in range(fs):
+            part = lax.dot_general(
+                hidden, og[:, j * dc:(j + 1) * dc], (((0,), (0,)), ((), ())),
+                preferred_element_type=jnp.float32)
+            for h in range(2):
+                own[2 * u + h, j // 2, j % 2] = part[h * ch:(h + 1) * ch]
+                xs[2 * u + h, j // 2, j % 2] = part[half + h * ch:half + (h + 1) * ch].astype(jnp.bfloat16)
+        x_copy(2 * u).start()
+        x_copy(2 * u + 1).start()
+
+    def backward(u):
+        cols = unit_cols(u)
+        for k in range(2):
+            for src in range(nz):
+                wy_copy(2 * u + k, src).wait_recv()
+        gate_in = pg[:, cols].astype(jnp.float32)
+        linear_in = pln[:, cols].astype(jnp.float32)
+        taps_gate, taps_linear = tg_ref[:, cols], tl_ref[:, cols]
+        gate_pre = conv_chunk(gate_in, taps_gate, bg_ref[:, cols])
+        linear_pre = conv_chunk(linear_in, taps_linear, bl_ref[:, cols])
+        sigma = jax.nn.sigmoid(gate_pre)
+        grad_hidden = jnp.zeros((tokens, unit), jnp.float32)
+        for j in range(fs):
+            grad_hidden += lax.dot_general(
+                og[:, j * dc:(j + 1) * dc], wbuf[j, cols], (((1,), (1,)), ((), ())),
+                preferred_element_type=jnp.float32)
+        grad_gate_pre = grad_hidden * linear_pre * sigma * (1.0 + gate_pre * (1.0 - sigma))
+        grad_linear_pre = grad_hidden * (gate_pre * sigma)
+        gg_ref[:, cols] = conv_back_chunk(grad_gate_pre, taps_gate).astype(jnp.bfloat16)
+        gl_ref[:, cols] = conv_back_chunk(grad_linear_pre, taps_linear).astype(jnp.bfloat16)
+        for j in range(3):
+            cpl[j:j + 1, cols] = jnp.sum(
+                grad_gate_pre * shift_down(gate_in, 2 - j), axis=0, keepdims=True)
+            cpl[j + 3:j + 4, cols] = jnp.sum(
+                grad_linear_pre * shift_down(linear_in, 2 - j), axis=0, keepdims=True)
+        cpl[6:7, cols] = jnp.sum(grad_gate_pre, axis=0, keepdims=True)
+        cpl[7:8, cols] = jnp.sum(grad_linear_pre, axis=0, keepdims=True)
+        count = unit // span
+        for b in range(count):
+            k = lax.rem(u * count + b - flat + peers, peers)
+
+            @pl.when(k != 0)
+            def _():
+                c_copy(k).start()
+
+    def weights(t):
+        @pl.when(t < chunks)
+        def _():
+            @pl.when(z < nz - 1)
+            def _():
+                wz_copy(0, t, z).start()
+
+            @pl.when(z > 0)
+            def _():
+                wz_copy(1, t, z).start()
+
+            wy_copy(t, z).start()
+
+        for d in range(1, nz):
+            k = t - d
+            live = (k >= 0) & (k < chunks)
+
+            @pl.when(live & (z >= d))
+            def _():
+                wz_copy(0, k, z - d).wait_recv()
+
+                @pl.when(z < nz - 1)
+                def _():
+                    wz_copy(0, k, z - d).start()
+
+                wy_copy(k, z - d).start()
+
+            @pl.when(live & (z + d < nz))
+            def _():
+                wz_copy(1, k, z + d).wait_recv()
+
+                @pl.when(z > 0)
+                def _():
+                    wz_copy(1, k, z + d).start()
+
+                wy_copy(k, z + d).start()
+
+    def add_step(c, s):
+        up = z + nz - s
+        down = z - nz + s
+
+        @pl.when(z <= s - 1)
+        def _():
+            total = own[c, up] + xr[c, up].astype(jnp.float32)
+
+            @pl.when(z > 0)
+            def _():
+                z_up(c, up).wait_recv()
+                zb[c, up] = (total + zb[c, up].astype(jnp.float32)).astype(jnp.bfloat16)
+
+            @pl.when(z == 0)
+            def _():
+                zb[c, up] = total.astype(jnp.bfloat16)
+
+            z_up(c, up).start()
+
+        @pl.when(z >= nz - s)
+        def _():
+            total = own[c, down] + xr[c, down].astype(jnp.float32)
+
+            @pl.when(z < nz - 1)
+            def _():
+                z_down(c, down).wait_recv()
+                zb[c, down] = (total + zb[c, down].astype(jnp.float32)).astype(jnp.bfloat16)
+
+            @pl.when(z == nz - 1)
+            def _():
+                zb[c, down] = total.astype(jnp.bfloat16)
+
+            z_down(c, down).start()
+
+    def line_end(c):
+        own[c, z] += xr[c, z].astype(jnp.float32)
+
+        @pl.when(z > 0)
+        def _():
+            z_up(c, z).wait_recv()
+            own[c, z] += zb[c, z].astype(jnp.float32)
+
+        @pl.when(z < nz - 1)
+        def _():
+            z_down(c, z).wait_recv()
+            own[c, z] += zb[c, nz].astype(jnp.float32)
+
+        ys[c] = own[c, z, 1 - y].astype(jnp.bfloat16)
+        y_copy(c).start()
+
+    def finish(c):
+        y_copy(c).wait_recv()
+        gd_ref[chunk_rows(c, rep)] = own[c, z, y] + yr[c].astype(jnp.float32)
+        a_copy(c).start()
+
+        @pl.when(c % 2 == 1)
+        def _():
+            u = c // 2
+            total = gd_ref[half_cols(u, rep)]
+            square = total * total
+            while square.shape[1] % 256 == 0:
+                middle = square.shape[1] // 2
+                square = square[:, :middle] + square[:, middle:]
+            rnb[flat, pl.ds(u, 1)] = jnp.sum(square.T, axis=0, keepdims=True)
+
+    ticks = chunks + nz + 1
+
+    @pl.loop(0, ticks)
+    def _(t):
+        weights(t)
+
+        c = t - 1 - nz
+
+        @pl.when((c >= 0) & (c < chunks))
+        def _():
+            finish(c)
+
+        c = t - nz
+
+        @pl.when((c >= 0) & (c < chunks))
+        def _():
+            line_end(c)
+
+        for s in range(nz - 1, 0, -1):
+            c = t - s
+
+            @pl.when((c >= 0) & (c < chunks))
+            def _():
+                if s == 1:
+                    x_copy(c).wait_recv()
+                add_step(c, s)
+
+        @pl.when(t < units)
+        def _():
+            @pl.when(t == 0)
+            def _():
+                og_copy().wait()
+
+            forward(t)
+
+        late = t - nz - 1
+
+        @pl.when((late >= 0) & (late % 2 == 0) & (late < chunks))
+        def _():
+            backward(late // 2)
+
+    @pl.loop(1, peers)
+    def _(k):
+        n_copy(k).start()
+
+    cpr[flat] = cpl[:, my_span()]
+
+    @pl.loop(1, peers)
+    def _(k):
+        c_copy(k).wait_recv()
+
+    sums = cpr[0]
+    for j in range(1, peers):
+        sums += cpr[j]
+    cps[...] = sums
+    cp_ref[:, my_span()] = sums
+
+    @pl.loop(1, peers)
+    def _(k):
+        b_copy(k).start()
+
+    @pl.loop(1, peers)
+    def _(k):
+        n_copy(k).wait_recv()
+
+    for side in range(2):
+        norms = rnb[side * fs]
+        for j in range(1, fs):
+            norms += rnb[side * fs + j]
+        rn_ref[:, side * half:(side + 1) * half] = norms
+
+    @pl.loop(1, peers)
+    def _(k):
+        b_copy(k).wait_recv()
+
+    @pl.loop(0, chunks)
+    def _(c):
+        a_copy(c).wait_recv()
+
+    @pl.loop(1, peers)
+    def _(k):
+        n_copy(k).wait_send()
+        c_copy(k).wait_send()
+        b_copy(k).wait_send()
+
+    @pl.loop(0, chunks)
+    def _(c):
+        x_copy(c).wait_send()
+        y_copy(c).wait_send()
+        a_copy(c).wait_send()
+
+        @pl.loop(0, nz)
+        def _(i):
+            @pl.when(i > z)
+            def _():
+                z_up(c, i).wait_send()
+
+            @pl.when(i < z)
+            def _():
+                z_down(c, i).wait_send()
+
+            wy_copy(c, i).wait_send()
+
+            @pl.when((i <= z) & (z < nz - 1))
+            def _():
+                wz_copy(0, c, i).wait_send()
+
+            @pl.when((i >= z) & (z > 0))
+            def _():
+                wz_copy(1, c, i).wait_send()
+
+
+def line_local(
+    fs, pre_gate, pre_linear, taps_gate, taps_linear, bias_gate, bias_linear, down_weight, out_grad
+):
+    tokens, ff = pre_gate.shape
+    dc = down_weight.shape[1]
+    unit = 256
+    units = ff // unit
+    chunks = 2 * units
+    ch = unit // 4
+    nz = fs // 2
+    peers = 2 * fs
+    f32, bf16 = jnp.float32, jnp.bfloat16
+    vmem = pl.BlockSpec(memory_space=pltpu.VMEM)
+    hbm = pl.BlockSpec(memory_space=pl.ANY)
+    dma = pltpu.SemaphoreType.DMA
+    gg, gl, cp, gd, rn = pl.pallas_call(
+        functools.partial(line_kernel, fs, unit),
+        out_shape=(
+            pltpu.VMEM((tokens, ff), bf16),
+            pltpu.VMEM((tokens, ff), bf16),
+            pltpu.VMEM((8, ff), f32),
+            pltpu.VMEM((ff, dc), f32),
+            pltpu.VMEM((units, unit), f32),
+        ),
+        in_specs=[hbm, hbm, vmem, vmem, vmem, vmem, hbm, hbm],
+        out_specs=(vmem,) * 5,
+        scratch_shapes=[
+            pltpu.VMEM((tokens, out_grad.shape[1]), bf16),
+            pltpu.VMEM((tokens, ff), bf16),
+            pltpu.VMEM((tokens, ff), bf16),
+            pltpu.VMEM((fs, ff, dc), bf16),
+            pltpu.VMEM((chunks, nz, 2, ch, dc), bf16),
+            pltpu.VMEM((chunks, nz, 2, ch, dc), bf16),
+            pltpu.VMEM((chunks, nz, 2, ch, dc), f32),
+            pltpu.VMEM((chunks, nz + 1, 2, ch, dc), bf16),
+            pltpu.VMEM((chunks, ch, dc), bf16),
+            pltpu.VMEM((chunks, ch, dc), bf16),
+            pltpu.VMEM((8, ff), f32),
+            pltpu.VMEM((peers, 8, ff // peers), f32),
+            pltpu.VMEM((8, ff // peers), f32),
+            pltpu.VMEM((peers, units, unit // 2), f32),
+            dma((2, units)), dma, dma,
+            dma((chunks,)), dma((chunks,)),
+            dma((2, chunks, nz)), dma((chunks, nz)), dma((chunks, nz)), dma((chunks, nz)),
+            dma((chunks, nz)), dma((chunks, nz)), dma((chunks, nz)), dma((chunks, nz)),
+            dma((chunks,)), dma((chunks,)), dma((chunks,)), dma((chunks,)),
+            dma((peers,)), dma((peers,)), dma((peers,)), dma((peers,)), dma((peers,)), dma((peers,)),
+        ],
+        compiler_params=pltpu.CompilerParams(
+            collective_id=0, has_side_effects=True, vmem_limit_bytes=55 << 20),
+    )(pre_gate, pre_linear, taps_gate, taps_linear, bias_gate[None], bias_linear[None],
+      down_weight, out_grad)
+    return put_out(gg, gl, cp, gd, rn)
+
+
+def on_a_line(fs, ff, dc):
+    nz = fs // 2
+    return fs % 2 == 0 and 2 <= nz <= 4 and ff % (256 * fs) == 0 and dc % 128 == 0
+
+
+def local(fs, *args):
+    if on_a_line(fs, args[0].shape[1], args[6].shape[1]):
+        return line_local(fs, *args)
+    return direct_local(fs, *args)
+
+
 def solution(mesh):
     in_specs = (
         P(("rep", "fs"), "tp"),

time: 189 us -> 149 us (0.79)
  Pallas kernels: 188 us -> 148 us
    pallas_call x1, Pallas kernels: 184 us -> 144 us  [line_local(): pl.pallas_call(functools.partial(line_kernel, fs, unit), out_shape=(pltpu...]
where the time goes in v2:
time: 149 us; the launch traced here: 148 us
  Pallas kernels  148 us (99%)
    pallas_call x1, Pallas kernels, line_local(): pl.pallas_call(functools.partial(line_kernel, fs, unit), out_shape=(pltpu...  144 us
    pallas_call x1, Pallas kernels, put_out(): pl.pallas_call(out_kernel, out_shape=(jax.ShapeDtypeStruct(gg.shape, gg.d...  4.05 us

profile of v2, /device:TPU:0, one launch (start us, length us, event | category | flops | bytes accessed | tf_op | source)
XLA Modules:
  0.0 148.4 jit_solution(7172311379918054273)
XLA Ops:
  0.6 143.7 %shard_map.143 = (bf16[768,2048]{1,0:T(8,128)(2,1)S(1)}, bf16[768,2048]{1,0:T(8,128)(2,1)S(1)}, f32[8,2048]{1,0:T(8,128)S(1)}, f32[2048,256]{1,0:T(8,128)S(1)}, f32[8,256]{1,0:T(8,128)S(1)}) custom-call(bf16[768,2048]{1,0:T(8,128)(2,1)} %pg_hbm.1, bf16[768,2048]{1,0:T(8,128)(2,1)} %pl_hbm.1, f32[3,2048]{1,0:T(4,128)} %tg_ref.1, f32[3,2048]{1,0:T(4,128)} %tl_ref.1, ...), custom_call_target="tpu_custom_call" | custom-call | tf_op jit(solution)/shard_map/pallas_call | solution.py:799
  144.4 4.1 %shard_map.144 = (bf16[768,2048]{1,0:T(8,128)(2,1)}, bf16[768,2048]{1,0:T(8,128)(2,1)}, f32[3,2048]{1,0:T(4,128)}, f32[3,2048]{1,0:T(4,128)}, f32[1,2048]{1,0:T(...) custom-call(bf16[768,2048]{1,0:T(8,128)(2,1)S(1)} %get-tuple-element.21.gg, ...), custom_call_target="tpu_custom_call" | custom-call | tf_op jit(solution)/shard_map/pallas_call | solution.py:335

commit v3 on v2

--- a/solution.py
+++ b/solution.py
@@ -396,7 +396,7 @@
     gg_ref, gl_ref, cp_ref, gd_ref, rn_ref,
     og, pg, pln, wbuf, xs, xr, own, zb, ys, yr, cpl, cpr, cps, rnb,
     in_sem, og_sem, w_sem, x_send, x_recv, wz_send, wz_recv, wy_send, wy_recv,
-    zu_send, zu_recv, zd_send, zd_recv, y_send, y_recv, a_send, a_recv,
+    z_send, z_recv, y_send, y_recv, a_send, a_recv,
     c_send, c_recv, b_send, b_recv, n_send, n_recv,
 ):
     me = lax.axis_index("fs")
@@ -452,46 +452,56 @@
         return pltpu.make_async_copy(w_hbm, wbuf.at[me], w_sem)
 
     def x_copy(c):
-        return remote(xs.at[c], xr.at[c], x_send.at[c], x_recv.at[c], {"rep": partner})
+        return remote(xs.at[c], xr.at[c], x_send, x_recv.at[c], {"rep": partner})
 
     def wz_copy(way, k, src):
         block = wbuf.at[src * 2 + y, w_rows(k)]
         to = z + 1 if way == 0 else z - 1
-        return remote(block, block, wz_send.at[way, k, src], wz_recv.at[k, src], {"fs": to * 2 + y})
+        return remote(block, block, wz_send, wz_recv.at[k, src], {"fs": to * 2 + y})
 
     def wy_copy(k, src):
         block = wbuf.at[src * 2 + y, w_rows(k)]
-        return remote(block, block, wy_send.at[k, src], wy_recv.at[k, src], {"fs": mate})
+        return remote(block, block, wy_send, wy_recv.at[k // 2], {"fs": mate})
 
     def z_up(c, i):
         return remote(
-            zb.at[c, i], zb.at[c, i], zu_send.at[c, i], zu_recv.at[c, i], {"fs": (z + 1) * 2 + y})
+            zb.at[c, i], zb.at[c, i], z_send, z_recv.at[c, i], {"fs": (z + 1) * 2 + y})
 
     def z_down(c, i):
         slot = jnp.where(i == z - 1, nz, i)
         return remote(
-            zb.at[c, i], zb.at[c, slot], zd_send.at[c, i], zd_recv.at[c, i], {"fs": (z - 1) * 2 + y})
+            zb.at[c, i], zb.at[c, slot], z_send, z_recv.at[c, slot], {"fs": (z - 1) * 2 + y})
+
+    def z_arrived(c, slot):
+        block = zb.at[c, slot]
+        remote(block, block, z_send, z_recv.at[c, slot], {"fs": mate}).wait_recv()
+
+    def all_sent(block, send):
+        remote(block, block, send, x_recv.at[0], {"fs": mate}).wait_send()
+
+    def all_arrived(block, recv):
+        remote(block, block, x_send, recv, {"fs": mate}).wait_recv()
 
     def y_copy(c):
-        return remote(ys.at[c], yr.at[c], y_send.at[c], y_recv.at[c], {"fs": mate})
+        return remote(ys.at[c], yr.at[c], y_send, y_recv.at[c], {"fs": mate})
 
     def a_copy(c):
         rows = chunk_rows(c, rep)
-        return remote(gd_ref.at[rows], gd_ref.at[rows], a_send.at[c], a_recv.at[c], {"rep": partner})
+        return remote(gd_ref.at[rows], gd_ref.at[rows], a_send, a_recv, {"rep": partner})
 
     def c_copy(k):
         at = lax.rem(flat + k, peers)
         cols = pl.ds(pl.multiple_of(at * span, span), span)
-        return remote(cpl.at[:, cols], cpr.at[flat], c_send.at[k], c_recv.at[k], peer(k))
+        return remote(cpl.at[:, cols], cpr.at[flat], c_send, c_recv, peer(k))
 
     def my_span():
         return pl.ds(pl.multiple_of(flat * span, span), span)
 
     def b_copy(k):
-        return remote(cps, cp_ref.at[:, my_span()], b_send.at[k], b_recv.at[k], peer(k))
+        return remote(cps, cp_ref.at[:, my_span()], b_send, b_recv, peer(k))
 
     def n_copy(k):
-        return remote(rnb.at[flat], rnb.at[flat], n_send.at[k], n_recv.at[k], peer(k))
+        return remote(rnb.at[flat], rnb.at[flat], n_send, n_recv, peer(k))
 
     barrier = pltpu.get_barrier_semaphore()
 
@@ -508,9 +518,6 @@
     def _(u):
         for copy in in_copies(u):
             copy.start()
-
-    w_copy().wait()
-    pl.semaphore_wait(barrier, peers - 1)
 
     def hidden_half(cols):
         gate_pre = conv_chunk(pg[:, cols].astype(jnp.float32), tg_ref[:, cols], bg_ref[:, cols])
@@ -529,14 +536,9 @@
             for h in range(2):
                 own[2 * u + h, j // 2, j % 2] = part[h * ch:(h + 1) * ch]
                 xs[2 * u + h, j // 2, j % 2] = part[half + h * ch:half + (h + 1) * ch].astype(jnp.bfloat16)
-        x_copy(2 * u).start()
-        x_copy(2 * u + 1).start()
-
     def backward(u):
         cols = unit_cols(u)
-        for k in range(2):
-            for src in range(nz):
-                wy_copy(2 * u + k, src).wait_recv()
+        all_arrived(wbuf.at[pl.ds(0, nz), cols], wy_recv.at[u])
         gate_in = pg[:, cols].astype(jnp.float32)
         linear_in = pln[:, cols].astype(jnp.float32)
         taps_gate, taps_linear = tg_ref[:, cols], tl_ref[:, cols]
@@ -614,7 +616,7 @@
 
             @pl.when(z > 0)
             def _():
-                z_up(c, up).wait_recv()
+                z_arrived(c, up)
                 zb[c, up] = (total + zb[c, up].astype(jnp.float32)).astype(jnp.bfloat16)
 
             @pl.when(z == 0)
@@ -629,7 +631,7 @@
 
             @pl.when(z < nz - 1)
             def _():
-                z_down(c, down).wait_recv()
+                z_arrived(c, down)
                 zb[c, down] = (total + zb[c, down].astype(jnp.float32)).astype(jnp.bfloat16)
 
             @pl.when(z == nz - 1)
@@ -643,12 +645,12 @@
 
         @pl.when(z > 0)
         def _():
-            z_up(c, z).wait_recv()
+            z_arrived(c, z)
             own[c, z] += zb[c, z].astype(jnp.float32)
 
         @pl.when(z < nz - 1)
         def _():
-            z_down(c, z).wait_recv()
+            z_arrived(c, nz)
             own[c, z] += zb[c, nz].astype(jnp.float32)
 
         ys[c] = own[c, z, 1 - y].astype(jnp.bfloat16)
@@ -669,26 +671,52 @@
                 square = square[:, :middle] + square[:, middle:]
             rnb[flat, pl.ds(u, 1)] = jnp.sum(square.T, axis=0, keepdims=True)
 
-    ticks = chunks + nz + 1
+    lag = 2
+    back_lag = 5
+    ticks = chunks + lag + nz
+
+    def send_half(u):
+        x_copy(2 * u).start()
+        x_copy(2 * u + 1).start()
+
+    def reduce_params():
+        cpr[flat] = cpl[:, my_span()]
+
+        all_arrived(cpr.at[pl.ds(0, peers - 1)], c_recv)
+        sums = cpr[0]
+        for j in range(1, peers):
+            sums += cpr[j]
+        cps[...] = sums
+        cp_ref[:, my_span()] = sums
+
+        @pl.loop(1, peers)
+        def _(k):
+            b_copy(k).start()
+
+    og_copy().wait()
+    forward(0)
+    w_copy().wait()
+    pl.semaphore_wait(barrier, peers - 1)
+    send_half(0)
 
     @pl.loop(0, ticks)
     def _(t):
         weights(t)
 
-        c = t - 1 - nz
+        c = t - lag - nz
 
         @pl.when((c >= 0) & (c < chunks))
         def _():
             finish(c)
 
-        c = t - nz
+        c = t - lag - nz + 1
 
         @pl.when((c >= 0) & (c < chunks))
         def _():
             line_end(c)
 
         for s in range(nz - 1, 0, -1):
-            c = t - s
+            c = t - lag - s + 1
 
             @pl.when((c >= 0) & (c < chunks))
             def _():
@@ -696,43 +724,40 @@
                     x_copy(c).wait_recv()
                 add_step(c, s)
 
-        @pl.when(t < units)
-        def _():
-            @pl.when(t == 0)
-            def _():
-                og_copy().wait()
-
-            forward(t)
-
-        late = t - nz - 1
+        @pl.when(t < units - 1)
+        def _():
+            forward(t + 1)
+            send_half(t + 1)
+
+        late = t - back_lag
 
         @pl.when((late >= 0) & (late % 2 == 0) & (late < chunks))
         def _():
             backward(late // 2)
 
+        @pl.when(t == ticks - 1)
+        def _():
+            reduce_params()
+
     @pl.loop(1, peers)
     def _(k):
         n_copy(k).start()
 
-    cpr[flat] = cpl[:, my_span()]
-
-    @pl.loop(1, peers)
-    def _(k):
-        c_copy(k).wait_recv()
-
-    sums = cpr[0]
-    for j in range(1, peers):
-        sums += cpr[j]
-    cps[...] = sums
-    cp_ref[:, my_span()] = sums
-
-    @pl.loop(1, peers)
-    def _(k):
-        b_copy(k).start()
-
-    @pl.loop(1, peers)
-    def _(k):
-        n_copy(k).wait_recv()
+    all_sent(xs, x_send)
+    all_sent(ys, y_send)
+    all_sent(zb.at[:, pl.ds(0, nz - 1)], z_send)
+    all_sent(wbuf.at[pl.ds(0, nz)], wy_send)
+
+    @pl.when((z == 0) | (z == nz - 1))
+    def _():
+        all_sent(wbuf.at[0], wz_send)
+
+    @pl.when((z > 0) & (z < nz - 1))
+    def _():
+        all_sent(wbuf.at[pl.ds(0, nz + 1)], wz_send)
+
+    all_sent(cpr.at[pl.ds(0, peers - 1)], c_send)
+    all_arrived(rnb.at[pl.ds(0, peers - 1)], n_recv)
 
     for side in range(2):
         norms = rnb[side * fs]
@@ -740,45 +765,11 @@
             norms += rnb[side * fs + j]
         rn_ref[:, side * half:(side + 1) * half] = norms
 
-    @pl.loop(1, peers)
-    def _(k):
-        b_copy(k).wait_recv()
-
-    @pl.loop(0, chunks)
-    def _(c):
-        a_copy(c).wait_recv()
-
-    @pl.loop(1, peers)
-    def _(k):
-        n_copy(k).wait_send()
-        c_copy(k).wait_send()
-        b_copy(k).wait_send()
-
-    @pl.loop(0, chunks)
-    def _(c):
-        x_copy(c).wait_send()
-        y_copy(c).wait_send()
-        a_copy(c).wait_send()
-
-        @pl.loop(0, nz)
-        def _(i):
-            @pl.when(i > z)
-            def _():
-                z_up(c, i).wait_send()
-
-            @pl.when(i < z)
-            def _():
-                z_down(c, i).wait_send()
-
-            wy_copy(c, i).wait_send()
-
-            @pl.when((i <= z) & (z < nz - 1))
-            def _():
-                wz_copy(0, c, i).wait_send()
-
-            @pl.when((i >= z) & (z > 0))
-            def _():
-                wz_copy(1, c, i).wait_send()
+    all_arrived(cpr.at[pl.ds(0, peers - 1)], b_recv)
+    all_arrived(gd_ref.at[pl.ds(0, ff // 2)], a_recv)
+    all_sent(gd_ref.at[pl.ds(0, ff // 2)], a_send)
+    all_sent(cpr.at[pl.ds(0, peers - 1)], b_send)
+    all_sent(rnb.at[pl.ds(0, peers - 1)], n_send)
 
 
 def line_local(
@@ -823,11 +814,9 @@
             pltpu.VMEM((8, ff // peers), f32),
             pltpu.VMEM((peers, units, unit // 2), f32),
             dma((2, units)), dma, dma,
-            dma((chunks,)), dma((chunks,)),
-            dma((2, chunks, nz)), dma((chunks, nz)), dma((chunks, nz)), dma((chunks, nz)),
-            dma((chunks, nz)), dma((chunks, nz)), dma((chunks, nz)), dma((chunks, nz)),
-            dma((chunks,)), dma((chunks,)), dma((chunks,)), dma((chunks,)),
-            dma((peers,)), dma((peers,)), dma((peers,)), dma((peers,)), dma((peers,)), dma((peers,)),
+            dma, dma((chunks,)), dma, dma((chunks, nz)), dma, dma((units,)),
+            dma, dma((chunks, nz + 1)), dma, dma((chunks,)), dma, dma,
+            dma, dma, dma, dma, dma, dma,
         ],
         compiler_params=pltpu.CompilerParams(
             collective_id=0, has_side_effects=True, vmem_limit_bytes=55 << 20),

time: 149 us -> 137 us (0.919)
  Pallas kernels: 148 us -> 137 us
    pallas_call x1, Pallas kernels: 144 us -> 133 us  [line_local(): pl.pallas_call(functools.partial(line_kernel, fs, unit), out_shape=(pltpu...]
where the time goes in v3:
time: 137 us
  Pallas kernels  137 us (100%)
    pallas_call x1, Pallas kernels, line_local(): pl.pallas_call(functools.partial(line_kernel, fs, unit), out_shape=(pltpu...  133 us
    pallas_call x1, Pallas kernels, put_out(): pl.pallas_call(out_kernel, out_shape=(jax.ShapeDtypeStruct(gg.shape, gg.d...  4.05 us

profile of v3, /device:TPU:0, one launch (start us, length us, event | category | flops | bytes accessed | tf_op | source)
XLA Modules:
  0.0 137.2 jit_solution(11247515192190172995)
XLA Ops:
  0.6 132.5 %shard_map.143 = (bf16[768,2048]{1,0:T(8,128)(2,1)S(1)}, bf16[768,2048]{1,0:T(8,128)(2,1)S(1)}, f32[8,2048]{1,0:T(8,128)S(1)}, f32[2048,256]{1,0:T(8,128)S(1)}, f32[8,256]{1,0:T(8,128)S(1)}) custom-call(bf16[768,2048]{1,0:T(8,128)(2,1)} %pg_hbm.1, bf16[768,2048]{1,0:T(8,128)(2,1)} %pl_hbm.1, f32[3,2048]{1,0:T(4,128)} %tg_ref.1, f32[3,2048]{1,0:T(4,128)} %tl_ref.1, ...), custom_call_target="tpu_custom_call" | custom-call | tf_op jit(solution)/shard_map/pallas_call | solution.py:790
  133.2 4.1 %shard_map.144 = (bf16[768,2048]{1,0:T(8,128)(2,1)}, bf16[768,2048]{1,0:T(8,128)(2,1)}, f32[3,2048]{1,0:T(4,128)}, f32[3,2048]{1,0:T(4,128)}, f32[1,2048]{1,0:T(...) custom-call(bf16[768,2048]{1,0:T(8,128)(2,1)S(1)} %get-tuple-element.21.gg, ...), custom_call_target="tpu_custom_call" | custom-call | tf_op jit(solution)/shard_map/pallas_call | solution.py:335

commit v4 on v3

--- a/solution.py
+++ b/solution.py
@@ -394,10 +394,10 @@
     fs, unit,
     pg_hbm, pl_hbm, tg_ref, tl_ref, bg_ref, bl_ref, w_hbm, og_hbm,
     gg_ref, gl_ref, cp_ref, gd_ref, rn_ref,
-    og, pg, pln, wbuf, xs, xr, own, zb, ys, yr, cpl, cpr, cps, rnb,
+    og, pg, pln, wbuf, xs, xr, own, zb, ys, yr, fsum, fr, cpl, cpr, nrm, blk, tail,
     in_sem, og_sem, w_sem, x_send, x_recv, wz_send, wz_recv, wy_send, wy_recv,
-    z_send, z_recv, y_send, y_recv, a_send, a_recv,
-    c_send, c_recv, b_send, b_recv, n_send, n_recv,
+    z_send, z_recv, y_send, y_recv, a_send, a_recv, f_send, f_recv,
+    c_send, c_recv, b_send, b_recv, t_send, t_recv,
 ):
     me = lax.axis_index("fs")
     rep = lax.axis_index("rep")
@@ -413,8 +413,11 @@
     units = ff // unit
     half = unit // 2
     chunks = 2 * units
+    split = chunks - 2
+    spare = chunks + 2
     ch = half // 2
     span = ff // peers
+    owners = (units - 1) * unit // span
     wch = unit // 2
 
     def unit_cols(u):
@@ -489,6 +492,9 @@
         rows = chunk_rows(c, rep)
         return remote(gd_ref.at[rows], gd_ref.at[rows], a_send, a_recv, {"rep": partner})
 
+    def f_copy(f):
+        return remote(fsum.at[f], fr.at[f], f_send, f_recv, {"rep": partner})
+
     def c_copy(k):
         at = lax.rem(flat + k, peers)
         cols = pl.ds(pl.multiple_of(at * span, span), span)
@@ -498,10 +504,10 @@
         return pl.ds(pl.multiple_of(flat * span, span), span)
 
     def b_copy(k):
-        return remote(cps, cp_ref.at[:, my_span()], b_send, b_recv, peer(k))
-
-    def n_copy(k):
-        return remote(rnb.at[flat], rnb.at[flat], n_send, n_recv, peer(k))
+        return remote(blk.at[flat], blk.at[flat], b_send, b_recv, peer(k))
+
+    def t_copy(k):
+        return remote(tail.at[flat], tail.at[flat], t_send, t_recv, peer(k))
 
     barrier = pltpu.get_barrier_semaphore()
 
@@ -527,6 +533,9 @@
     def forward(u):
         for copy in in_copies(u):
             copy.wait()
+        last = u == units - 1
+        mine_at = jnp.where(last, split + 2 * rep, 2 * u)
+        theirs_at = jnp.where(last, split + 2 * partner, spare)
         hidden = jnp.concatenate(
             [hidden_half(half_cols(u, rep)), hidden_half(half_cols(u, partner))], axis=1)
         for j in range(fs):
@@ -534,8 +543,10 @@
                 hidden, og[:, j * dc:(j + 1) * dc], (((0,), (0,)), ((), ())),
                 preferred_element_type=jnp.float32)
             for h in range(2):
-                own[2 * u + h, j // 2, j % 2] = part[h * ch:(h + 1) * ch]
-                xs[2 * u + h, j // 2, j % 2] = part[half + h * ch:half + (h + 1) * ch].astype(jnp.bfloat16)
+                theirs = part[half + h * ch:half + (h + 1) * ch]
+                own[mine_at + h, j // 2, j % 2] = part[h * ch:(h + 1) * ch]
+                own[theirs_at + h, j // 2, j % 2] = theirs
+                xs[2 * u + h, j // 2, j % 2] = theirs.astype(jnp.bfloat16)
     def backward(u):
         cols = unit_cols(u)
         all_arrived(wbuf.at[pl.ds(0, nz), cols], wy_recv.at[u])
@@ -565,25 +576,30 @@
         for b in range(count):
             k = lax.rem(u * count + b - flat + peers, peers)
 
-            @pl.when(k != 0)
+            @pl.when((k != 0) & (u < units - 1))
             def _():
                 c_copy(k).start()
 
+    def own_z(k):
+        @pl.when(z < nz - 1)
+        def _():
+            wz_copy(0, k, z).start()
+
+        @pl.when(z > 0)
+        def _():
+            wz_copy(1, k, z).start()
+
     def weights(t):
-        @pl.when(t < chunks)
-        def _():
-            @pl.when(z < nz - 1)
-            def _():
-                wz_copy(0, t, z).start()
-
-            @pl.when(z > 0)
-            def _():
-                wz_copy(1, t, z).start()
-
-            wy_copy(t, z).start()
+        @pl.when(t + ahead_z < chunks)
+        def _():
+            own_z(t + ahead_z)
+
+        @pl.when(t + ahead_y < chunks)
+        def _():
+            wy_copy(t + ahead_y, z).start()
 
         for d in range(1, nz):
-            k = t - d
+            k = t - d + early
             live = (k >= 0) & (k < chunks)
 
             @pl.when(live & (z >= d))
@@ -612,7 +628,7 @@
 
         @pl.when(z <= s - 1)
         def _():
-            total = own[c, up] + xr[c, up].astype(jnp.float32)
+            total = own[c, up]
 
             @pl.when(z > 0)
             def _():
@@ -627,7 +643,7 @@
 
         @pl.when(z >= nz - s)
         def _():
-            total = own[c, down] + xr[c, down].astype(jnp.float32)
+            total = own[c, down]
 
             @pl.when(z < nz - 1)
             def _():
@@ -641,8 +657,6 @@
             z_down(c, down).start()
 
     def line_end(c):
-        own[c, z] += xr[c, z].astype(jnp.float32)
-
         @pl.when(z > 0)
         def _():
             z_arrived(c, z)
@@ -663,17 +677,35 @@
 
         @pl.when(c % 2 == 1)
         def _():
-            u = c // 2
-            total = gd_ref[half_cols(u, rep)]
-            square = total * total
-            while square.shape[1] % 256 == 0:
-                middle = square.shape[1] // 2
-                square = square[:, :middle] + square[:, middle:]
-            rnb[flat, pl.ds(u, 1)] = jnp.sum(square.T, axis=0, keepdims=True)
+            norms_of(c // 2)
+
+    def norms_of(u):
+        total = gd_ref[half_cols(u, rep)]
+        square = total * total
+        while square.shape[1] % 256 == 0:
+            middle = square.shape[1] // 2
+            square = square[:, :middle] + square[:, middle:]
+        nrm[pl.ds(u, 1)] = jnp.sum(square.T, axis=0, keepdims=True)
+
+    def finish_both(f):
+        c = split + f
+        y_copy(c).wait_recv()
+        fsum[f] = own[c, z, y] + yr[c].astype(jnp.float32)
+        f_copy(f).start()
+
+    def join_both():
+        all_arrived(fr, f_recv)
+        for f in range(4):
+            rows = chunk_rows(split + f % 2, f // 2)
+            gd_ref[rows] = fsum[f] + fr[f]
+        norms_of(units - 1)
 
     lag = 2
     back_lag = 5
-    ticks = chunks + lag + nz
+    ahead_y = 3
+    early = 0
+    ahead_z = 1
+    ticks = max(split + lag + nz, chunks - 1 + back_lag)
 
     def send_half(u):
         x_copy(2 * u).start()
@@ -686,64 +718,93 @@
         sums = cpr[0]
         for j in range(1, peers):
             sums += cpr[j]
-        cps[...] = sums
-        cp_ref[:, my_span()] = sums
+        blk[flat] = sums
 
         @pl.loop(1, peers)
         def _(k):
             b_copy(k).start()
 
+    w_copy().wait()
+    tail[flat] = jnp.zeros(tail.shape[1:], jnp.float32)
+    pl.semaphore_wait(barrier, peers - 1)
+    for k in range(ahead_z):
+        own_z(k)
+    for k in range(ahead_y):
+        wy_copy(k, z).start()
     og_copy().wait()
     forward(0)
-    w_copy().wait()
-    pl.semaphore_wait(barrier, peers - 1)
     send_half(0)
 
     @pl.loop(0, ticks)
     def _(t):
         weights(t)
 
+        late = t - back_lag
+
+        @pl.when((late >= 0) & (late % 2 == 0) & (late < chunks))
+        def _():
+            backward(late // 2)
+
         c = t - lag - nz
 
-        @pl.when((c >= 0) & (c < chunks))
+        @pl.when((c >= 0) & (c < split))
         def _():
             finish(c)
 
         c = t - lag - nz + 1
 
-        @pl.when((c >= 0) & (c < chunks))
+        @pl.when((c >= 0) & (c < split))
         def _():
             line_end(c)
 
         for s in range(nz - 1, 0, -1):
             c = t - lag - s + 1
 
-            @pl.when((c >= 0) & (c < chunks))
+            @pl.when((c >= 0) & (c < split))
             def _():
                 if s == 1:
                     x_copy(c).wait_recv()
+                    own[c] += xr[c].astype(jnp.float32)
                 add_step(c, s)
 
+        @pl.loop(0, 4)
+        def _(f):
+            s = t - 2 * f
+
+            @pl.when(s == nz + 1)
+            def _():
+                finish_both(f)
+
+            @pl.when(s == nz)
+            def _():
+                line_end(split + f)
+
+            @pl.when((s >= 1) & (s < nz))
+            def _():
+                add_step(split + f, s)
+
         @pl.when(t < units - 1)
         def _():
-            forward(t + 1)
-            send_half(t + 1)
-
-        late = t - back_lag
-
-        @pl.when((late >= 0) & (late % 2 == 0) & (late < chunks))
-        def _():
-            backward(late // 2)
-
-        @pl.when(t == ticks - 1)
+            forward(jnp.where(t == 0, units - 1, t))
+
+            @pl.when(t > 0)
+            def _():
+                send_half(t)
+
+        @pl.when((t == ticks - 2) & (flat < owners))
         def _():
             reduce_params()
+
+    join_both()
+    tail[flat, 0:8] = cpl[:, ff - unit:]
+    tail[flat, 8:, 0:half] = nrm[...]
 
     @pl.loop(1, peers)
     def _(k):
-        n_copy(k).start()
-
-    all_sent(xs, x_send)
+        t_copy(k).start()
+
+    all_sent(xs.at[pl.ds(0, split)], x_send)
+    all_sent(fsum, f_send)
     all_sent(ys, y_send)
     all_sent(zb.at[:, pl.ds(0, nz - 1)], z_send)
     all_sent(wbuf.at[pl.ds(0, nz)], wy_send)
@@ -756,20 +817,33 @@
     def _():
         all_sent(wbuf.at[pl.ds(0, nz + 1)], wz_send)
 
-    all_sent(cpr.at[pl.ds(0, peers - 1)], c_send)
-    all_arrived(rnb.at[pl.ds(0, peers - 1)], n_recv)
-
+    @pl.when(flat < owners)
+    def _():
+        all_sent(cpr.at[pl.ds(0, owners - 1)], c_send)
+        all_sent(blk.at[pl.ds(0, peers - 1)], b_send)
+        all_arrived(blk.at[pl.ds(0, owners - 1)], b_recv)
+
+    @pl.when(flat >= owners)
+    def _():
+        all_sent(cpr.at[pl.ds(0, owners)], c_send)
+        all_arrived(blk.at[pl.ds(0, owners)], b_recv)
+
+    for q in range(owners):
+        cp_ref[:, q * span:(q + 1) * span] = blk[q]
+    all_arrived(tail.at[pl.ds(0, peers - 1)], t_recv)
+    sums = tail[0, 0:8]
+    for q in range(1, peers):
+        sums += tail[q, 0:8]
+    cp_ref[:, ff - unit:] = sums
     for side in range(2):
-        norms = rnb[side * fs]
+        norms = tail[side * fs, 8:, 0:half]
         for j in range(1, fs):
-            norms += rnb[side * fs + j]
+            norms += tail[side * fs + j, 8:, 0:half]
         rn_ref[:, side * half:(side + 1) * half] = norms
 
-    all_arrived(cpr.at[pl.ds(0, peers - 1)], b_recv)
-    all_arrived(gd_ref.at[pl.ds(0, ff // 2)], a_recv)
-    all_sent(gd_ref.at[pl.ds(0, ff // 2)], a_send)
-    all_sent(cpr.at[pl.ds(0, peers - 1)], b_send)
-    all_sent(rnb.at[pl.ds(0, peers - 1)], n_send)
+    all_arrived(gd_ref.at[pl.ds(0, split * ch)], a_recv)
+    all_sent(gd_ref.at[pl.ds(0, split * ch)], a_send)
+    all_sent(tail.at[pl.ds(0, peers - 1)], t_send)
 
 
 def line_local(
@@ -804,18 +878,21 @@
             pltpu.VMEM((tokens, ff), bf16),
             pltpu.VMEM((fs, ff, dc), bf16),
             pltpu.VMEM((chunks, nz, 2, ch, dc), bf16),
-            pltpu.VMEM((chunks, nz, 2, ch, dc), bf16),
-            pltpu.VMEM((chunks, nz, 2, ch, dc), f32),
-            pltpu.VMEM((chunks, nz + 1, 2, ch, dc), bf16),
-            pltpu.VMEM((chunks, ch, dc), bf16),
-            pltpu.VMEM((chunks, ch, dc), bf16),
+            pltpu.VMEM((chunks - 2, nz, 2, ch, dc), bf16),
+            pltpu.VMEM((chunks + 4, nz, 2, ch, dc), f32),
+            pltpu.VMEM((chunks + 2, nz + 1, 2, ch, dc), bf16),
+            pltpu.VMEM((chunks + 2, ch, dc), bf16),
+            pltpu.VMEM((chunks + 2, ch, dc), bf16),
+            pltpu.VMEM((4, ch, dc), f32),
+            pltpu.VMEM((4, ch, dc), f32),
             pltpu.VMEM((8, ff), f32),
             pltpu.VMEM((peers, 8, ff // peers), f32),
-            pltpu.VMEM((8, ff // peers), f32),
-            pltpu.VMEM((peers, units, unit // 2), f32),
+            pltpu.VMEM((units, unit // 2), f32),
+            pltpu.VMEM((peers, 8, ff // peers), f32),
+            pltpu.VMEM((peers, 8 + units, unit), f32),
             dma((2, units)), dma, dma,
             dma, dma((chunks,)), dma, dma((chunks, nz)), dma, dma((units,)),
-            dma, dma((chunks, nz + 1)), dma, dma((chunks,)), dma, dma,
+            dma, dma((chunks + 2, nz + 1)), dma, dma((chunks + 2,)), dma, dma, dma, dma,
             dma, dma, dma, dma, dma, dma,
         ],
         compiler_params=pltpu.CompilerParams(

time: 137 us -> 132 us (0.964)
  Pallas kernels: 137 us -> 131 us
    pallas_call x1, Pallas kernels: 133 us -> 127 us  [line_local(): pl.pallas_call(functools.partial(line_kernel, fs, unit), out_shape=(pltpu...]
where the time goes in v4:
time: 132 us; the launch traced here: 131 us
  Pallas kernels  131 us (99%)
    pallas_call x1, Pallas kernels, line_local(): pl.pallas_call(functools.partial(line_kernel, fs, unit), out_shape=(pltpu...  127 us
    pallas_call x1, Pallas kernels, put_out(): pl.pallas_call(out_kernel, out_shape=(jax.ShapeDtypeStruct(gg.shape, gg.d...  4.05 us

profile of v4, /device:TPU:0, one launch (start us, length us, event | category | flops | bytes accessed | tf_op | source)
XLA Modules:
  0.0 131.4 jit_solution(6895356350574852809)
XLA Ops:
  0.6 126.8 %shard_map.143 = (bf16[768,2048]{1,0:T(8,128)(2,1)S(1)}, bf16[768,2048]{1,0:T(8,128)(2,1)S(1)}, f32[8,2048]{1,0:T(8,128)S(1)}, f32[2048,256]{1,0:T(8,128)S(1)}, f32[8,256]{1,0:T(8,128)S(1)}) custom-call(bf16[768,2048]{1,0:T(8,128)(2,1)} %pg_hbm.1, bf16[768,2048]{1,0:T(8,128)(2,1)} %pl_hbm.1, f32[3,2048]{1,0:T(4,128)} %tg_ref.1, f32[3,2048]{1,0:T(4,128)} %tl_ref.1, ...), custom_call_target="tpu_custom_call" | custom-call | tf_op jit(solution)/shard_map/pallas_call | solution.py:864
  127.4 4.1 %shard_map.144 = (bf16[768,2048]{1,0:T(8,128)(2,1)}, bf16[768,2048]{1,0:T(8,128)(2,1)}, f32[3,2048]{1,0:T(4,128)}, f32[3,2048]{1,0:T(4,128)}, f32[1,2048]{1,0:T(...) custom-call(bf16[768,2048]{1,0:T(8,128)(2,1)S(1)} %get-tuple-element.21.gg, ...), custom_call_target="tpu_custom_call" | custom-call | tf_op jit(solution)/shard_map/pallas_call | solution.py:335

commit v5 on v4

--- a/solution.py
+++ b/solution.py
@@ -308,10 +308,13 @@
 
 
 def out_kernel(gg, gl, cp, gd, rn, ogg, ogl, otg, otl, obg, obl, ogd, orn, sem):
-    copies = [
-        pltpu.make_async_copy(source, target, sem.at[i])
-        for i, (source, target) in enumerate(((gg, ogg), (gl, ogl), (gd, ogd)))
-    ]
+    parts = sem.shape[1]
+    copies = []
+    for i, (source, target) in enumerate(((gg, ogg), (gl, ogl), (gd, ogd))):
+        size = source.shape[0] // parts
+        for j in range(parts):
+            rows = pl.ds(j * size, size)
+            copies.append(pltpu.make_async_copy(source.at[rows], target.at[rows], sem.at[i, j]))
     for copy in copies:
         copy.start()
     otg[...] = cp[0:3]
@@ -339,7 +342,7 @@
             taps, taps, row, row, jax.ShapeDtypeStruct(gd.shape, gd.dtype), row),
         in_specs=[vmem] * 5,
         out_specs=(hbm, hbm, vmem, vmem, vmem, vmem, hbm, vmem),
-        scratch_shapes=[pltpu.SemaphoreType.DMA((3,))],
+        scratch_shapes=[pltpu.SemaphoreType.DMA((3, 4))],
         compiler_params=pltpu.CompilerParams(vmem_limit_bytes=2 << 20),
     )(*[pltpu.with_memory_space_constraint(value, pltpu.VMEM) for value in (gg, gl, cp, gd, rn)])
     return ogg, ogl, otg, otl, obg[0], obl[0], ogd, orn[0]
@@ -599,7 +602,7 @@
             wy_copy(t + ahead_y, z).start()
 
         for d in range(1, nz):
-            k = t - d + early
+            k = t - d
             live = (k >= 0) & (k < chunks)
 
             @pl.when(live & (z >= d))
@@ -702,9 +705,8 @@
 
     lag = 2
     back_lag = 5
-    ahead_y = 3
-    early = 0
-    ahead_z = 1
+    ahead_y = 5
+    ahead_z = 2
     ticks = max(split + lag + nz, chunks - 1 + back_lag)
 
     def send_half(u):
@@ -739,7 +741,8 @@
     def _(t):
         weights(t)
 
-        late = t - back_lag
+        slack = jnp.where(t < units + back_lag + 1, 2, jnp.where(t < 2 * units + back_lag - 4, 1, 0))
+        late = t - back_lag - slack
 
         @pl.when((late >= 0) & (late % 2 == 0) & (late < chunks))
         def _():
@@ -904,7 +907,9 @@
 
 def on_a_line(fs, ff, dc):
     nz = fs // 2
-    return fs % 2 == 0 and 2 <= nz <= 4 and ff % (256 * fs) == 0 and dc % 128 == 0
+    return (
+        fs % 2 == 0 and 2 <= nz <= 4 and ff % (256 * fs) == 0
+        and 1536 <= ff <= 512 * fs and dc % 128 == 0)
 
 
 def local(fs, *args):

time: 132 us -> 130 us (0.985)
  no operation moved by 1% of the time
where the time goes in v5:
time: 130 us
  Pallas kernels  130 us (100%)
    pallas_call x1, Pallas kernels, line_local(): pl.pallas_call(functools.partial(line_kernel, fs, unit), out_shape=(pltpu...  125 us
    pallas_call x1, Pallas kernels, put_out(): pl.pallas_call(out_kernel, out_shape=(jax.ShapeDtypeStruct(gg.shape, gg.d...  4.03 us

profile of v5, /device:TPU:0, one launch (start us, length us, event | category | flops | bytes accessed | tf_op | source)
XLA Modules:
  0.0 130.1 jit_solution(8223276453675438352)
XLA Ops:
  0.6 125.5 %shard_map.143 = (bf16[768,2048]{1,0:T(8,128)(2,1)S(1)}, bf16[768,2048]{1,0:T(8,128)(2,1)S(1)}, f32[8,2048]{1,0:T(8,128)S(1)}, f32[2048,256]{1,0:T(8,128)S(1)}, f32[8,256]{1,0:T(8,128)S(1)}) custom-call(bf16[768,2048]{1,0:T(8,128)(2,1)} %pg_hbm.1, bf16[768,2048]{1,0:T(8,128)(2,1)} %pl_hbm.1, f32[3,2048]{1,0:T(4,128)} %tg_ref.1, f32[3,2048]{1,0:T(4,128)} %tl_ref.1, ...), custom_call_target="tpu_custom_call" | custom-call | tf_op jit(solution)/shard_map/pallas_call | solution.py:867
  126.1 4.0 %shard_map.144 = (bf16[768,2048]{1,0:T(8,128)(2,1)}, bf16[768,2048]{1,0:T(8,128)(2,1)}, f32[3,2048]{1,0:T(4,128)}, f32[3,2048]{1,0:T(4,128)}, f32[1,2048]{1,0:T(...) custom-call(bf16[768,2048]{1,0:T(8,128)(2,1)S(1)} %get-tuple-element.21.gg, ...), custom_call_target="tpu_custom_call" | custom-call | tf_op jit(solution)/shard_map/pallas_call | solution.py:338
